TPU v7x, 256 devices: a whole 4x4x8 slice. The times are simulated.
256 devices in a mesh: ep: 16 (over y, x), tp: 16 (over z, core).
Axes of the slice: x: 4, y: 4, z: 8, core: 2. Of those that a mesh axis runs over, the one named last changes fastest.
Arguments:
- mix_tokens: bfloat16 [16384, 1, 1024], P(('ep', 'tp')), may hold values from -6 to 6
- mix_gain: float32 [1024], replicated, may hold values from 0.1 to 1.9
- w_query: bfloat16 [1024, 1024], replicated, may hold values from -0.1875 to 0.1875
- w_key: bfloat16 [1024, 256], replicated, may hold values from -0.1875 to 0.1875
- w_value: bfloat16 [1024, 256], replicated, may hold values from -0.1875 to 0.1875
- query_gain: float32 [64], replicated, may hold values from 1.2 to 14
- key_gain: float32 [64], replicated, may hold values from 1.2 to 14
- w_out: bfloat16 [1024, 1024], replicated, may hold values from -0.1875 to 0.1875
- expert_tokens: bfloat16 [32768, 1024], P(('ep', 'tp')), may hold values from -6 to 6
- expert_gain: float32 [1024], replicated, may hold values from 0.1 to 1.9
- route_ids: int32 [32768, 2], P(('ep', 'tp')), may hold values from 0 to 31, all different within a row; in each aligned block of 128 rows (0 to 127, 128 to 255, ...) at most 9 rows name the same one
- route_weights: float32 [32768, 2], P(('ep', 'tp')), may hold values from 0.1 to 1
- w_gate: bfloat16 [32, 1024, 4096], P('ep', None, 'tp'), may hold values from -0.1875 to 0.1875
- w_up: bfloat16 [32, 1024, 4096], P('ep', None, 'tp'), may hold values from -0.1875 to 0.1875
- w_down: bfloat16 [32, 4096, 1024], P('ep', 'tp'), may hold values from -0.09375 to 0.09375
Outputs:
- mix_out: bfloat16 [16384, 1, 1024], P(('ep', 'tp'))
- experts_out: bfloat16 [32768, 1024], P(('ep', 'tp'))
Inputs may be any that keep to these rules, and one draw needn't show every extreme that they name: `route_ids`: each row names 2 different experts. Among the rows of one device no expert is named more than 9 times, and in every draw some expert is named exactly 9 times by the rows of some device.
All inputs are finite; a program needn't handle non-finite values.
Results may differ from a plain program's by a relative error of at most 0.018.
The roundings to bfloat16 on the way count: a program that leaves them out, or rounds other values in their place, can miss the bound.
Values may be sent and summed in bfloat16 or wider, within the bound.
A program may use at most 128 MiB of HBM per device.

v0:
```python
import math
import jax
import jax.numpy as jnp
from jax import lax
from jax.sharding import PartitionSpec as P

HEAD = 64
GRID_W = 64
epsilon = 1e-06


def normalize(values, gain_vec):
    widened = values.astype(jnp.float32)
    return (
        widened
        * lax.rsqrt(jnp.mean(widened * widened, axis=-1, keepdims=True) + epsilon)
        * gain_vec
    )


def angle_tables(positions, head_size):
    quarter = head_size // 4
    frequency = 10000.0 ** (-jnp.arange(quarter, dtype=jnp.float32) / quarter)
    grid_pos = jnp.stack([positions // GRID_W, positions % GRID_W], axis=-1).astype(jnp.float32)
    angles = grid_pos[:, :, None] * frequency[None, None, :]
    return (jnp.cos(angles), jnp.sin(angles))


def turn(values, cosine_table, sine_table):
    shaped = values.shape
    quarter = shaped[-1] // 4
    leading = (shaped[0],) + (1,) * (len(shaped) - 2) + (2, quarter)
    cosine_table = cosine_table.reshape(leading)
    sine_table = sine_table.reshape(leading)
    halves = values.reshape(shaped[:-1] + (2, 2, quarter))
    first_part = halves[..., 0, :]
    second_part = halves[..., 1, :]
    turned = jnp.stack(
        [
            first_part * cosine_table - second_part * sine_table,
            first_part * sine_table + second_part * cosine_table,
        ],
        axis=-2,
    )
    return turned.reshape(shaped)


def attend(queries, fold_state, key_piece):
    key_rows = key_piece.shape[0]
    block_rows = math.gcd(key_rows, 1024)
    blocks = key_piece.reshape((key_rows // block_rows, block_rows) + key_piece.shape[1:])
    score_scale = HEAD ** (-0.5)

    def step_block(carried, block_keys):
        running_max, totals, accumulated = carried
        keys_part = block_keys[..., :HEAD]
        values_part = block_keys[..., HEAD:]
        scores = (
            jnp.einsum("qshd,ksd->qshk", queries, keys_part, preferred_element_type=jnp.float32)
            * score_scale
        )
        new_max = jnp.maximum(running_max, jnp.max(scores, axis=-1))
        shrink = jnp.exp(running_max - new_max)
        raised = jnp.exp(scores - new_max[..., None])
        totals = totals * shrink + jnp.sum(raised, axis=-1)
        accumulated = accumulated * shrink[..., None] + jnp.einsum(
            "qshk,ksd->qshd",
            raised.astype(jnp.bfloat16),
            values_part,
            preferred_element_type=jnp.float32,
        )
        return ((new_max, totals, accumulated), None)

    return lax.scan(step_block, fold_state, blocks)[0]


def mixer_half(mix_tokens, mix_gain, w_query, w_key, w_value, query_gain, key_gain, w_out):
    tp_count = lax.axis_size("tp")
    seq_rows, sequences, model_width = mix_tokens.shape
    head_count = w_query.shape[1] // HEAD
    key_heads = w_key.shape[1] // HEAD
    local_heads = head_count // tp_count
    normed = normalize(mix_tokens, mix_gain).astype(jnp.bfloat16)
    queries = jnp.dot(normed, w_query, preferred_element_type=jnp.float32).astype(jnp.bfloat16)
    keys_raw = jnp.dot(normed, w_key, preferred_element_type=jnp.float32).astype(jnp.bfloat16)
    values = jnp.dot(normed, w_value, preferred_element_type=jnp.float32).astype(jnp.bfloat16)
    queries = queries.reshape(seq_rows, sequences, tp_count, local_heads * HEAD)
    key_value = jnp.concatenate(
        [
            keys_raw.reshape(seq_rows, sequences, key_heads, HEAD),
            values.reshape(seq_rows, sequences, key_heads, HEAD),
        ],
        axis=-1,
    )
    key_value = jnp.repeat(key_value, tp_count // key_heads, axis=2)
    packed = jnp.concatenate([queries, key_value], axis=-1)
    arrived = lax.all_to_all(packed, "tp", split_axis=2, concat_axis=0, tiled=True)
    span_rows = arrived.shape[0]
    positions = lax.axis_index("ep") * span_rows + jnp.arange(span_rows, dtype=jnp.int32)
    cosine_table, sine_table = angle_tables(positions, HEAD)
    query_width = local_heads * HEAD
    own_queries = normalize(
        arrived[:, :, 0, :query_width].reshape(span_rows, sequences, local_heads, HEAD), query_gain
    )
    own_queries = turn(own_queries, cosine_table, sine_table).astype(jnp.bfloat16)
    own_keys = normalize(arrived[:, :, 0, query_width : query_width + HEAD], key_gain)
    own_keys = turn(own_keys, cosine_table, sine_table).astype(jnp.bfloat16)
    key_pairs = jnp.concatenate([own_keys, arrived[:, :, 0, query_width + HEAD :]], axis=-1)
    start_state = (
        jnp.full((span_rows, sequences, local_heads), -1e30, jnp.float32),
        jnp.zeros((span_rows, sequences, local_heads), jnp.float32),
        jnp.zeros((span_rows, sequences, local_heads, HEAD), jnp.float32),
    )
    running_max, totals, accumulated = attend(
        own_queries, start_state, lax.all_gather(key_pairs, "ep", axis=0, tiled=True)
    )
    mixed = (
        (accumulated / totals[..., None])
        .astype(jnp.bfloat16)
        .reshape(span_rows, sequences, query_width)
    )
    returned = lax.all_to_all(mixed, "tp", split_axis=0, concat_axis=2, tiled=True)
    return jnp.dot(returned, w_out, preferred_element_type=jnp.float32).astype(jnp.bfloat16)


def joint_hidden(w_gate, w_up, piece_rows):
    gate_act = jnp.einsum("rjd,jdf->rjf", piece_rows, w_gate, preferred_element_type=jnp.float32)
    up_act = jnp.einsum("rjd,jdf->rjf", piece_rows, w_up, preferred_element_type=jnp.float32)
    return (jax.nn.silu(gate_act) * up_act).astype(jnp.bfloat16)


def joint_down(hidden_all, w_down):
    group_sum = jnp.einsum(
        "rjf,jfd->rjd", hidden_all, w_down, preferred_element_type=jnp.float32
    ).astype(jnp.bfloat16)
    return lax.optimization_barrier(group_sum).astype(jnp.float32)


def expert_half(expert_tokens, expert_gain, route_ids, route_weights, w_gate, w_up, w_down):
    ep_count = lax.axis_size("ep")
    tok_count, model_width = expert_tokens.shape
    top_count = route_ids.shape[1]
    local_experts = w_gate.shape[0]
    expert_count = local_experts * ep_count
    capacity = tok_count * top_count * 9 // (8 * expert_count)
    slot_count = ep_count * capacity * local_experts
    normed = normalize(expert_tokens, expert_gain).astype(jnp.bfloat16)
    flat_ids = route_ids.reshape(-1)
    matches = (flat_ids[:, None] == jnp.arange(expert_count, dtype=jnp.int32)[None, :]).astype(
        jnp.int32
    )
    rank_ids = jnp.sum((jnp.cumsum(matches, axis=0) - 1) * matches, axis=1)
    slot_ids = (
        flat_ids // local_experts * capacity + rank_ids
    ) * local_experts + flat_ids % local_experts
    chosen = slot_ids.reshape(tok_count, top_count)
    dispatch = jnp.sum(
        (chosen[:, :, None] == jnp.arange(slot_count, dtype=jnp.int32)[None, None, :]).astype(
            jnp.bfloat16
        ),
        axis=1,
    )
    outgoing = lax.dot_general(
        dispatch, normed, (((0,), (0,)), ((), ())), preferred_element_type=jnp.float32
    )
    outgoing = outgoing.astype(jnp.bfloat16).reshape(ep_count, capacity, local_experts, model_width)
    incoming = lax.all_to_all(outgoing, "ep", split_axis=0, concat_axis=0, tiled=True)
    own_rows = ep_count * capacity
    incoming = incoming.reshape(own_rows, local_experts, model_width)
    hidden_all = joint_hidden(w_gate, w_up, lax.all_gather(incoming, "tp", axis=0, tiled=True))
    summed = lax.psum_scatter(
        joint_down(hidden_all, w_down).astype(jnp.bfloat16), "tp", scatter_dimension=0, tiled=True
    )
    expert_results = summed.reshape(ep_count, capacity, local_experts, model_width)
    returned = lax.all_to_all(
        expert_results, "ep", split_axis=0, concat_axis=0, tiled=True
    ).reshape(slot_count, model_width)
    picked = jnp.take(returned, slot_ids, axis=0).reshape(tok_count, top_count, model_width)
    combined = jnp.sum(route_weights[:, :, None] * picked.astype(jnp.float32), axis=1)
    return combined.astype(jnp.bfloat16)


def body(
    mix_tokens,
    mix_gain,
    w_query,
    w_key,
    w_value,
    query_gain,
    key_gain,
    w_out,
    expert_tokens,
    expert_gain,
    route_ids,
    route_weights,
    w_gate,
    w_up,
    w_down,
):
    mix_out = mixer_half(mix_tokens, mix_gain, w_query, w_key, w_value, query_gain, key_gain, w_out)
    experts_out = expert_half(
        expert_tokens, expert_gain, route_ids, route_weights, w_gate, w_up, w_down
    )
    return (mix_out, experts_out)


def solution(mesh):
    placed = (
        P(("ep", "tp"), None, None),
        P(),
        P(),
        P(),
        P(),
        P(),
        P(),
        P(),
        P(("ep", "tp"), None),
        P(),
        P(("ep", "tp"), None),
        P(("ep", "tp"), None),
        P("ep", None, "tp"),
        P("ep", None, "tp"),
        P("ep", "tp", None),
    )
    return jax.shard_map(
        body,
        mesh=mesh,
        in_specs=placed,
        out_specs=(P(("ep", "tp"), None, None), P(("ep", "tp"), None)),
        check_vma=False,
    )
```

profile of v0, /device:TPU:1, one launch (start us, length us, event | category | flops | bytes accessed | tf_op | source)
XLA Modules:
  0.0 339.7 jit_solution(8806245419591874709)
XLA Ops:
  10.4 1.1 fusion.21
  11.5 1.3 convolution_convert_fusion
  13.0 18.7 %all_to_all.43 = bf16[16,9,2,1024]{3,2,1,0:T(2,128)(2,1)S(1)} all-to-all(bf16[16,9,2,1024]{3,2,1,0:T(2,128)(2,1)S(1)} %reshape.571), channel_id=1, replica_groups=mesh['ep'=16,'tp'=16] {'ep'}, dimensions={0} | all-to-all | bytes 1179648 | tf_op jit(solution)/shard_map/all_to_all | solution.py:167
  32.9 1.3 convolution_convert_fusion.4
  34.3 1.3 convolution_convert_fusion.3
  36.7 1.0 pad_maximum_fusion
  37.7 10.4 %all-to-all-start = ((bf16[64,1,16,192]{3,0,1,2:T(8,128)(2,1)}), bf16[64,1,16,192]{3,0,1,2:T(8,128)(2,1)S(1)}, u32[]{:S(2)}, u32[]{:S(2)}) async-start(bf16[64,1,16,192]{3,0,1,2:T(8,128)(2,1)} %pad_maximum_fusion), calls=%async_computation | async-start | bytes 1048576 | tf_op jit(solution)/shard_map/all_to_all | solution.py:97
  48.3 22.1 %all-to-all-done = bf16[64,1,16,192]{3,0,1,2:T(8,128)(2,1)S(1)} async-done(((bf16[64,1,16,192]{3,0,1,2:T(8,128)(2,1)}), bf16[64,1,16,192]{3,0,1,2:T(8,128)(2,1)S(1)}, u32[]{:S(2)}, u32[]{:S(2)}) %all-to-all-start) | async-done | bytes 393248 | tf_op jit(solution)/shard_map/all_to_all | solution.py:97
  72.4 1.1 multiply_multiply_fusion
  75.4 1.1 copy.151
  77.2 28.6 %all-gather.5.cloned.1.call-done = bf16[2304,2,1024]{2,0,1:T(8,128)(2,1)} async-done(((bf16[144,2,1024]{2,0,1:T(8,128)(2,1)}), bf16[2304,2,1024]{2,0,1:T(8,128)(2,1)}) %all-gather.5.cloned.1.call-update) | async-done | bytes 9437200 | tf_op jit(solution)/shard_map/all_gather | solution.py:170
  105.8 8.7 %convolution_bitcast_fusion.1 = f32[2304,2,256]{2,0,1:T(8,128)} fusion(bf16[2304,2,1024]{2,0,1:T(8,128)(2,1)} %all-gather.5.cloned.1.call-done, bf16[2,1024,256]{2,1,0:T(8,128)(2,1)} %param.29), kind=kOutput, calls=%fused_computation.26 | convolution fusion | flops 2415919104 | bytes 15204352 | tf_op jit(solution)/shard_map/rjd,jdf->rjf/dot_general | solution.py:127
  114.5 11.7 %convert_bitcast_fusion = bf16[2304,2,1024]{2,0,1:T(8,128)(2,1)} fusion(bf16[2,256,1024]{2,1,0:T(8,128)(2,1)} %param.31, bf16[2304,2,1024]{2,0,1:T(8,128)(2,1)} %all-gather.5.cloned.1.call-done, bf16[2,1024,256]{2,1,0:T(8,128)(2,1)} %param.30, f32[2304,2,256]{2,0,1:T(8,128)} %convolution_bitcast_fusion.1), kind=kOutput, calls=%fused_computation.23 | convolution fusion | flops 4843634688 | bytes 25690112 | tf_op jit(solution)/shard_map/rjf,jfd->rjd/dot_general | solution.py:133
  126.2 36.4 %all-gather.3.cloned.1.call-done = bf16[16384,1,128]{2,0,1:T(8,128)(2,1)} async-done(((bf16[1024,1,128]{2,0,1:T(8,128)(2,1)}), bf16[16384,1,128]{2,0,1:T(8,128)(2,1)}) %all-gather.3.cloned.1.call-update) | async-done | bytes 4194320 | tf_op jit(solution)/shard_map/all_gather | solution.py:115
  162.7 131.4 %while.15 = (s32[]{:T(128)}, f32[1024,1,1]{0,2,1:T(1,128)S(1)}, f32[1024,1,1]{0,2,1:T(1,128)S(1)}, f32[1024,1,1,64]{0,3,2,1:T(8,128)S(1)}, bf16[16,1024,1,128]{3...) while((s32[]{:T(128)}, f32[1024,1,1]{0,2,1:T(1,128)S(1)}, ...), condition=%wide.region_6.7_spmd.clone, body=%wide.region_3.6_spmd.clone.sunk | while | flops 277025792 | bytes 31129728 | solution.py:74
  162.7 1.0 dynamic-slice_bitcast_fusion.2
  163.6 2.7 multiply_reduce_fusion.4
  166.4 3.1 fusion.81
  170.8 1.0 dynamic-slice_bitcast_fusion.2
  171.7 2.7 multiply_reduce_fusion.4
  174.5 3.2 fusion.81
  180.3 2.7 multiply_reduce_fusion.4
  183.0 3.2 fusion.81
  187.6 1.0 dynamic-slice_bitcast_fusion.2
  188.6 2.7 multiply_reduce_fusion.4
  191.3 3.2 fusion.81
  195.9 1.0 dynamic-slice_bitcast_fusion.2
  196.9 2.7 multiply_reduce_fusion.4
  199.6 3.2 fusion.81
  204.2 1.0 dynamic-slice_bitcast_fusion.2
  205.2 2.7 multiply_reduce_fusion.4
  207.9 3.2 fusion.81
  213.5 2.7 multiply_reduce_fusion.4
  216.2 3.2 fusion.81
  220.8 1.0 dynamic-slice_bitcast_fusion.2
  221.8 2.7 multiply_reduce_fusion.4
  224.5 3.2 fusion.81
  229.1 1.0 dynamic-slice_bitcast_fusion.2
  230.1 2.7 multiply_reduce_fusion.4
  232.8 3.2 fusion.81
  237.4 1.0 dynamic-slice_bitcast_fusion.2
  238.3 2.7 multiply_reduce_fusion.4
  241.1 3.1 fusion.81
  245.5 1.0 dynamic-slice_bitcast_fusion.2
  246.4 2.7 multiply_reduce_fusion.4
  249.2 3.1 fusion.81
  254.5 2.7 multiply_reduce_fusion.4
  257.3 3.1 fusion.81
  262.6 2.7 multiply_reduce_fusion.4
  265.4 3.1 fusion.81
  270.7 2.7 multiply_reduce_fusion.4
  273.5 3.1 fusion.81
  278.8 2.7 multiply_reduce_fusion.4
  281.6 3.1 fusion.81
  286.9 2.7 multiply_reduce_fusion.4
  289.7 3.1 fusion.81
  296.4 7.9 %all-to-all-start.1 = ((bf16[16,2,2048]{2,1,0:T(2,128)(2,1)}), bf16[16,2,2048]{2,1,0:T(2,128)(2,1)S(1)}, u32[]{:S(2)}, u32[]{:S(2)}) async-start(bf16[16,2,2048]{2,1,0:T(2,128)(2,1)} %reshape.590), calls=%async_computation.1 | async-start | bytes 262144 | tf_op jit(solution)/shard_map/all_to_all | solution.py:122
  304.7 2.5 copy.149
  307.1 6.0 %all-to-all-done.1 = bf16[16,2,2048]{2,1,0:T(2,128)(2,1)S(1)} async-done(((bf16[16,2,2048]{2,1,0:T(2,128)(2,1)}), bf16[16,2,2048]{2,1,0:T(2,128)(2,1)S(1)}, u32[]{:S(2)}, u32[]{:S(2)}) %all-to-all-start.1) | async-done | bytes 131104 | tf_op jit(solution)/shard_map/all_to_all | solution.py:122
  313.1 4.2 %all-to-all-start.3 = ((bf16[16,9,2,1024]{3,2,1,0:T(2,128)(2,1)}), bf16[16,9,2,1024]{3,2,1,0:T(2,128)(2,1)S(1)}, u32[]{:S(2)}, u32[]{:S(2)}) async-start(bf16[16,9,2,1024]{3,2,1,0:T(2,128)(2,1)} %bitcast.24), calls=%async_computation.4 | async-start | bytes 1179648 | tf_op jit(solution)/shard_map/all_to_all | solution.py:175
  318.8 2.7 fusion.20
  321.5 7.7 %all-to-all-done.3 = bf16[16,9,2,1024]{3,2,1,0:T(2,128)(2,1)S(1)} async-done(((bf16[16,9,2,1024]{3,2,1,0:T(2,128)(2,1)}), bf16[16,9,2,1024]{3,2,1,0:T(2,128)(2,1)S(1)}, u32[]{:S(2)}, u32[]{:S(2)}) %all-to-all-start.3) | async-done | bytes 589856 | tf_op jit(solution)/shard_map/all_to_all | solution.py:175
  329.4 1.2 gather_fusion
  330.8 2.4 multiply_reduce_fusion.1
  (185 shorter events, 43.6 us)
Async XLA Ops:
  7.2 28.7 %copy-start = (bf16[1024,1024]{1,0:T(8,128)(2,1)S(1)}, bf16[1024,1024]{1,0:T(8,128)(2,1)}, u32[]{:S(2)}) copy-start(bf16[1024,1024]{1,0:T(8,128)(2,1)} %param.19) | copy-start | bytes 6291460
  7.2 25.5 %copy-start.2 = (bf16[64,1,1024]{2,0,1:T(8,128)(2,1)S(1)}, bf16[64,1,1024]{2,0,1:T(8,128)(2,1)}, u32[]{:S(2)}) copy-start(bf16[64,1,1024]{2,0,1:T(8,128)(2,1)} %param.17) | copy-start | bytes 393220
  7.2 25.7 %copy-start.3 = (f32[1024]{0:T(1024)S(1)}, f32[1024]{0:T(1024)}, u32[]{:S(2)}) copy-start(f32[1024]{0:T(1024)} %param.18) | copy-start | bytes 12292
  7.2 98.6 %all-gather.5.cloned.1.call-start = ((), (), s32[]{:S(2)}) async-start(), calls=%async_computation.6 | async-start | bytes 10027008 | tf_op jit(solution)/shard_map/all_gather | solution.py:170
  32.7 15.4 %copy-start.6 = (f32[64]{0:T(128)S(1)}, f32[64]{0:T(128)}, u32[]{:S(2)}) copy-start(f32[64]{0:T(128)} %param.23) | copy-start | bytes 772
  36.7 39.9 %copy-start.5 = (f32[64]{0:T(128)S(1)}, f32[64]{0:T(128)}, u32[]{:S(2)}) copy-start(f32[64]{0:T(128)} %param.22) | copy-start | bytes 772
  37.7 32.7 %all-to-all-start = ((bf16[64,1,16,192]{3,0,1,2:T(8,128)(2,1)}), bf16[64,1,16,192]{3,0,1,2:T(8,128)(2,1)S(1)}, u32[]{:S(2)}, u32[]{:S(2)}) async-start(bf16[64,1,16,192]{3,0,1,2:T(8,128)(2,1)} %pad_maximum_fusion), calls=%async_computation | async-start | bytes 1048576 | tf_op jit(solution)/shard_map/all_to_all | solution.py:97
  48.1 114.6 %all-gather.3.cloned.1.call-start = ((), (), s32[]{:S(2)}) async-start(), calls=%async_computation.5 | async-start | bytes 4456448 | tf_op jit(solution)/shard_map/all_gather | solution.py:115
  75.1 229.5 %reduce-scatter.2.cloned.1.call-start = ((), (), s32[]{:S(2)}) async-start(), calls=%async_computation.7 | async-start | bytes 10027008 | tf_op jit(solution)/shard_map/reduce_scatter | solution.py:171
  162.7 141.9 %copy-start.4 = (f32[128,2]{0,1:T(2,128)S(1)}, f32[128,2]{0,1:T(2,128)}, u32[]{:S(2)}) copy-start(f32[128,2]{0,1:T(2,128)} %param.28) | copy-start | bytes 3076
  166.4 3.4 %copy-start.1 = (f32[1024,1024]{1,0:T(8,128)S(1)}, f32[1024,1024]{1,0:T(8,128)}, u32[]{:S(2)}) copy-start(f32[1024,1024]{1,0:T(8,128)} %get-tuple-element.163) | copy-start | bytes 12582916 | tf_op jit(solution)/shard_map/while
  174.5 3.9 %copy-start.1 = (f32[1024,1024]{1,0:T(8,128)S(1)}, f32[1024,1024]{1,0:T(8,128)}, u32[]{:S(2)}) copy-start(f32[1024,1024]{1,0:T(8,128)} %get-tuple-element.163) | copy-start | bytes 12582916 | tf_op jit(solution)/shard_map/while
  183.0 3.6 %copy-start.1 = (f32[1024,1024]{1,0:T(8,128)S(1)}, f32[1024,1024]{1,0:T(8,128)}, u32[]{:S(2)}) copy-start(f32[1024,1024]{1,0:T(8,128)} %get-tuple-element.163) | copy-start | bytes 12582916 | tf_op jit(solution)/shard_map/while
  191.3 3.6 %copy-start.1 = (f32[1024,1024]{1,0:T(8,128)S(1)}, f32[1024,1024]{1,0:T(8,128)}, u32[]{:S(2)}) copy-start(f32[1024,1024]{1,0:T(8,128)} %get-tuple-element.163) | copy-start | bytes 12582916 | tf_op jit(solution)/shard_map/while
  199.6 3.6 %copy-start.1 = (f32[1024,1024]{1,0:T(8,128)S(1)}, f32[1024,1024]{1,0:T(8,128)}, u32[]{:S(2)}) copy-start(f32[1024,1024]{1,0:T(8,128)} %get-tuple-element.163) | copy-start | bytes 12582916 | tf_op jit(solution)/shard_map/while
  207.9 3.6 %copy-start.1 = (f32[1024,1024]{1,0:T(8,128)S(1)}, f32[1024,1024]{1,0:T(8,128)}, u32[]{:S(2)}) copy-start(f32[1024,1024]{1,0:T(8,128)} %get-tuple-element.163) | copy-start | bytes 12582916 | tf_op jit(solution)/shard_map/while
  216.2 3.6 %copy-start.1 = (f32[1024,1024]{1,0:T(8,128)S(1)}, f32[1024,1024]{1,0:T(8,128)}, u32[]{:S(2)}) copy-start(f32[1024,1024]{1,0:T(8,128)} %get-tuple-element.163) | copy-start | bytes 12582916 | tf_op jit(solution)/shard_map/while
  224.5 3.6 %copy-start.1 = (f32[1024,1024]{1,0:T(8,128)S(1)}, f32[1024,1024]{1,0:T(8,128)}, u32[]{:S(2)}) copy-start(f32[1024,1024]{1,0:T(8,128)} %get-tuple-element.163) | copy-start | bytes 12582916 | tf_op jit(solution)/shard_map/while
  232.8 3.6 %copy-start.1 = (f32[1024,1024]{1,0:T(8,128)S(1)}, f32[1024,1024]{1,0:T(8,128)}, u32[]{:S(2)}) copy-start(f32[1024,1024]{1,0:T(8,128)} %get-tuple-element.163) | copy-start | bytes 12582916 | tf_op jit(solution)/shard_map/while
  241.0 3.4 %copy-start.1 = (f32[1024,1024]{1,0:T(8,128)S(1)}, f32[1024,1024]{1,0:T(8,128)}, u32[]{:S(2)}) copy-start(f32[1024,1024]{1,0:T(8,128)} %get-tuple-element.163) | copy-start | bytes 12582916 | tf_op jit(solution)/shard_map/while
  249.1 3.4 %copy-start.1 = (f32[1024,1024]{1,0:T(8,128)S(1)}, f32[1024,1024]{1,0:T(8,128)}, u32[]{:S(2)}) copy-start(f32[1024,1024]{1,0:T(8,128)} %get-tuple-element.163) | copy-start | bytes 12582916 | tf_op jit(solution)/shard_map/while
  257.2 3.4 %copy-start.1 = (f32[1024,1024]{1,0:T(8,128)S(1)}, f32[1024,1024]{1,0:T(8,128)}, u32[]{:S(2)}) copy-start(f32[1024,1024]{1,0:T(8,128)} %get-tuple-element.163) | copy-start | bytes 12582916 | tf_op jit(solution)/shard_map/while
  265.4 3.4 %copy-start.1 = (f32[1024,1024]{1,0:T(8,128)S(1)}, f32[1024,1024]{1,0:T(8,128)}, u32[]{:S(2)}) copy-start(f32[1024,1024]{1,0:T(8,128)} %get-tuple-element.163) | copy-start | bytes 12582916 | tf_op jit(solution)/shard_map/while
  273.5 3.4 %copy-start.1 = (f32[1024,1024]{1,0:T(8,128)S(1)}, f32[1024,1024]{1,0:T(8,128)}, u32[]{:S(2)}) copy-start(f32[1024,1024]{1,0:T(8,128)} %get-tuple-element.163) | copy-start | bytes 12582916 | tf_op jit(solution)/shard_map/while
  281.6 3.4 %copy-start.1 = (f32[1024,1024]{1,0:T(8,128)S(1)}, f32[1024,1024]{1,0:T(8,128)}, u32[]{:S(2)}) copy-start(f32[1024,1024]{1,0:T(8,128)} %get-tuple-element.163) | copy-start | bytes 12582916 | tf_op jit(solution)/shard_map/while
  289.7 3.4 %copy-start.1 = (f32[1024,1024]{1,0:T(8,128)S(1)}, f32[1024,1024]{1,0:T(8,128)}, u32[]{:S(2)}) copy-start(f32[1024,1024]{1,0:T(8,128)} %get-tuple-element.163) | copy-start | bytes 12582916 | tf_op jit(solution)/shard_map/while
  296.4 16.8 %all-to-all-start.1 = ((bf16[16,2,2048]{2,1,0:T(2,128)(2,1)}), bf16[16,2,2048]{2,1,0:T(2,128)(2,1)S(1)}, u32[]{:S(2)}, u32[]{:S(2)}) async-start(bf16[16,2,2048]{2,1,0:T(2,128)(2,1)} %reshape.590), calls=%async_computation.1 | async-start | bytes 262144 | tf_op jit(solution)/shard_map/all_to_all | solution.py:122
  313.1 16.1 %all-to-all-start.3 = ((bf16[16,9,2,1024]{3,2,1,0:T(2,128)(2,1)}), bf16[16,9,2,1024]{3,2,1,0:T(2,128)(2,1)S(1)}, u32[]{:S(2)}, u32[]{:S(2)}) async-start(bf16[16,9,2,1024]{3,2,1,0:T(2,128)(2,1)} %bitcast.24), calls=%async_computation.4 | async-start | bytes 1179648 | tf_op jit(solution)/shard_map/all_to_all | solution.py:175
Sparse Core Ops, SparseCore 0:
  32.8 72.8 all-gather.4
  108.2 54.3 all-gather.2
  165.2 69.8 reduce-scatter.1
where the time goes:
time: 341 us; the launch traced here: 340 us
  waiting for transfers between devices  101 us (30%)
  matrix products  85.9 us (25%)
  other arithmetic  61.8 us (18%)
  local copies, waits for them, and re-layouts  35 us (10%)
  starting transfers between devices  22.7 us (7%)
  blocking collectives  18.7 us (5%)
  between operations  14.2 us (4%)
    reduce_sum x16, other arithmetic, step_block(): totals = totals * shrink + jnp.sum(raised, axis=-1)  50 us
    dot_general x16, matrix products, step_block(): jnp.einsum('qshd,ksd->qshk', queries, keys_part, preferred_element_type=j...  43.4 us
    all_gather x1, waiting for transfers between devices, mixer_half(): lax.all_gather(key_pairs, 'ep', axis=0, tiled=True)  36.4 us
    all_gather x1, waiting for transfers between devices, expert_half(): lax.all_gather(incoming, 'tp', axis=0, tiled=True)  28.6 us
    all_to_all x1, waiting for transfers between devices, mixer_half(): lax.all_to_all(packed, 'tp', split_axis=2, concat_axis=0, tiled=True)  22.1 us
    all_to_all x1, blocking collectives, expert_half(): lax.all_to_all(outgoing, 'ep', split_axis=0, concat_axis=0, tiled=True)  18.7 us
    squeeze x16, local copies, waits for them, and re-layouts, attend(): return lax.scan(step_block, fold_state, blocks)[0]  15.6 us
    dot_general x16, matrix products, step_block(): jnp.einsum('qshk,ksd->qshd', raised.astype(jnp.bfloat16), values_part, pr...  14.9 us
  transfers between devices with their start and end apart: 6, of which 5 were waited for; matrix products, arithmetic and copies ran while one was open for 49% of the time, Pallas kernels for 0%

commit v1 on v0

--- a/solution.py
+++ b/solution.py
@@ -167,7 +167,13 @@
     incoming = lax.all_to_all(outgoing, "ep", split_axis=0, concat_axis=0, tiled=True)
     own_rows = ep_count * capacity
     incoming = incoming.reshape(own_rows, local_experts, model_width)
-    hidden_all = joint_hidden(w_gate, w_up, lax.all_gather(incoming, "tp", axis=0, tiled=True))
+    hidden_all = joint_hidden(
+        w_gate,
+        w_up,
+        jnp.concatenate(
+            lax.all_to_all(jnp.stack([incoming] * lax.axis_size("tp")), "tp", 0, 0), axis=0
+        ),
+    )
     summed = lax.psum_scatter(
         joint_down(hidden_all, w_down).astype(jnp.bfloat16), "tp", scatter_dimension=0, tiled=True
     )

time: 341 us -> 482 us (1.41)
  waiting for transfers between devices: 101 us -> 239 us
  blocking collectives: 18.7 us -> 0 us
  local copies, waits for them, and re-layouts: 35 us -> 47.1 us
  starting transfers between devices: 22.7 us -> 32.6 us
    all_to_all x0 -> x2, waiting for transfers between devices: none -> 208 us  [the longest x1 201 us: expert_half(): lax.all_to_all(jnp.stack([incoming] * lax.axis_size('tp')), 'tp', 0, 0)]
    all_gather x1, waiting for transfers between devices: 36.4 us -> 0.02 us  [mixer_half(): lax.all_gather(key_pairs, 'ep', axis=0, tiled=True)]
    all_gather x1 -> x0, waiting for transfers between devices: 28.6 us -> none  [expert_half(): lax.all_gather(incoming, 'tp', axis=0, tiled=True)]
    all_to_all x1 -> x0, blocking collectives: 18.7 us -> none  [expert_half(): lax.all_to_all(outgoing, 'ep', split_axis=0, concat_axis=0, tiled=True)]
    all_to_all x0 -> x2, starting transfers between devices: none -> 12.4 us  [the longest x1 7.57 us: expert_half(): lax.all_to_all(outgoing, 'ep', split_axis=0, concat_axis=0, tiled=True)]
    all_to_all x0 -> x1, local copies, waits for them, and re-layouts: none -> 9.14 us  [expert_half(): lax.all_to_all(jnp.stack([incoming] * lax.axis_size('tp')), 'tp', 0, 0)]
    all_to_all x1, waiting for transfers between devices: 22.1 us -> 17.1 us  [mixer_half(): lax.all_to_all(packed, 'tp', split_axis=2, concat_axis=0, tiled=True)]
    another operation x2 -> x4, local copies, waits for them, and re-layouts: 0.2 us -> 5.2 us  [the longest x2 5 us: expert_half(): jnp.stack([incoming] * lax.axis_size('tp'))]
  transfers between devices with their start and end apart: 6 -> 7, of which waited for: 5 -> 5; matrix products, arithmetic and copies ran while one was open for 49% -> 35% of each run, Pallas kernels for 0% -> 0%
where the time goes in v1:
time: 482 us; the launch traced here: 481 us
  waiting for transfers between devices  239 us (50%)
  matrix products  85.4 us (18%)
  other arithmetic  59.9 us (12%)
  local copies, waits for them, and re-layouts  47.1 us (10%)
  starting transfers between devices  32.6 us (7%)
  between operations  16 us (3%)
    all_to_all x1, waiting for transfers between devices, expert_half(): lax.all_to_all(jnp.stack([incoming] * lax.axis_size('tp')), 'tp', 0, 0)  201 us
    reduce_sum x16, other arithmetic, step_block(): totals = totals * shrink + jnp.sum(raised, axis=-1)  49.7 us
    dot_general x16, matrix products, step_block(): jnp.einsum('qshd,ksd->qshk', queries, keys_part, preferred_element_type=j...  44.1 us
    all_to_all x1, waiting for transfers between devices, mixer_half(): lax.all_to_all(packed, 'tp', split_axis=2, concat_axis=0, tiled=True)  17.1 us
    squeeze x16, local copies, waits for them, and re-layouts, attend(): return lax.scan(step_block, fold_state, blocks)[0]  15.6 us
    dot_general x16, matrix products, step_block(): jnp.einsum('qshk,ksd->qshd', raised.astype(jnp.bfloat16), values_part, pr...  15 us
    dot_general x1, matrix products, joint_down(): jnp.einsum('rjf,jfd->rjd', hidden_all, w_down, preferred_element_type=jnp...  11.6 us
    all_to_all x1, starting transfers between devices, mixer_half(): lax.all_to_all(packed, 'tp', split_axis=2, concat_axis=0, tiled=True)  10.5 us
  transfers between devices with their start and end apart: 7, of which 5 were waited for; matrix products, arithmetic and copies ran while one was open for 35% of the time, Pallas kernels for 0%

profile of v1, /device:TPU:1, one launch (start us, length us, event | category | flops | bytes accessed | tf_op | source)
XLA Modules:
  0.0 480.6 jit_solution(12613687883258034145)
XLA Ops:
  11.2 1.1 fusion.21
  12.3 1.4 convolution_convert_fusion
  13.6 1.0 reshape.573
  14.7 7.6 %all-to-all-start.2 = ((bf16[16,9,2,1024]{3,2,1,0:T(2,128)(2,1)}), bf16[16,9,2,1024]{3,2,1,0:T(2,128)(2,1)S(1)}, u32[]{:S(2)}, u32[]{:S(2)}) async-start(bf16[16,9,2,1024]{3,2,1,0:T(2,128)(2,1)} %reshape.573), calls=%async_computation.2 | async-start | bytes 1179648 | tf_op jit(solution)/shard_map/all_to_all | solution.py:167
  22.7 1.3 convolution_convert_fusion.3
  25.2 1.0 pad_maximum_fusion
  26.2 7.2 %all-to-all-done.2 = bf16[16,9,2,1024]{3,2,1,0:T(2,128)(2,1)S(1)} async-done(((bf16[16,9,2,1024]{3,2,1,0:T(2,128)(2,1)}), bf16[16,9,2,1024]{3,2,1,0:T(2,128)(2,1)S(1)}, u32[]{:S(2)}, u32[]{:S(2)}) %all-to-all-start.2) | async-done | bytes 589856 | tf_op jit(solution)/shard_map/all_to_all | solution.py:167
  33.4 10.5 %all-to-all-start = ((bf16[64,1,16,192]{3,0,1,2:T(8,128)(2,1)}), bf16[64,1,16,192]{3,0,1,2:T(8,128)(2,1)S(1)}, u32[]{:S(2)}, u32[]{:S(2)}) async-start(bf16[64,1,16,192]{3,0,1,2:T(8,128)(2,1)} %pad_maximum_fusion), calls=%async_computation | async-start | bytes 1048576 | tf_op jit(solution)/shard_map/all_to_all | solution.py:97
  44.0 17.1 %all-to-all-done = bf16[64,1,16,192]{3,0,1,2:T(8,128)(2,1)S(1)} async-done(((bf16[64,1,16,192]{3,0,1,2:T(8,128)(2,1)}), bf16[64,1,16,192]{3,0,1,2:T(8,128)(2,1)S(1)}, u32[]{:S(2)}, u32[]{:S(2)}) %all-to-all-start) | async-done | bytes 393248 | tf_op jit(solution)/shard_map/all_to_all | solution.py:97
  61.1 4.9 %stack.23 = bf16[16,144,2,1024]{3,1,2,0:T(8,128)(2,1)} broadcast(bf16[144,2,1024]{2,0,1:T(8,128)(2,1)S(1)} %copy.151), dimensions={1,2,3} | broadcast | bytes 10027008 | tf_op jit(solution)/shard_map/stack | solution.py:174
  66.0 4.8 %all-to-all-start.3 = ((bf16[16,144,2,1024]{3,1,2,0:T(8,128)(2,1)}), bf16[16,144,2,1024]{3,1,2,0:T(8,128)(2,1)}, u32[]{:S(2)}, u32[]{:S(2)}) async-start(bf16[16,144,2,1024]{3,1,2,0:T(8,128)(2,1)} %stack.23), calls=%async_computation.3 | async-start | bytes 18874368 | tf_op jit(solution)/shard_map/all_to_all | solution.py:174
  74.6 200.8 %all-to-all-done.3 = bf16[16,144,2,1024]{3,1,2,0:T(8,128)(2,1)} async-done(((bf16[16,144,2,1024]{3,1,2,0:T(8,128)(2,1)}), bf16[16,144,2,1024]{3,1,2,0:T(8,128)(2,1)}, u32[]{:S(2)}, u32[]{:S(2)}) %all-to-all-start.3) | async-done | bytes 9437216 | tf_op jit(solution)/shard_map/all_to_all | solution.py:174
  275.3 9.1 %copy.152 = bf16[16,144,2,1024]{3,1,0,2:T(8,128)(2,1)} copy(bf16[16,144,2,1024]{3,1,2,0:T(8,128)(2,1)} %all-to-all-done.3) | data formatting | bytes 18874368 | tf_op jit(solution)/shard_map/all_to_all | solution.py:174
  284.5 8.5 %convolution_bitcast_fusion.1 = f32[2304,2,256]{2,0,1:T(8,128)} fusion(bf16[2304,2,1024]{2,0,1:T(8,128)(2,1)} %bitcast.150, bf16[2,1024,256]{2,1,0:T(8,128)(2,1)S(1)} %copy-done.9), kind=kOutput, calls=%fused_computation.26 | convolution fusion | flops 2415919104 | bytes 15204352 | tf_op jit(solution)/shard_map/rjd,jdf->rjf/dot_general | solution.py:127
  292.9 11.6 %convert_bitcast_fusion = bf16[2304,2,1024]{2,0,1:T(8,128)(2,1)} fusion(bf16[2,256,1024]{2,1,0:T(8,128)(2,1)} %param.31, bf16[2304,2,1024]{2,0,1:T(8,128)(2,1)} %bitcast.151, bf16[2,1024,256]{2,1,0:T(8,128)(2,1)} %param.30, f32[2304,2,256]{2,0,1:T(8,128)} %convolution_bitcast_fusion.1), kind=kOutput, calls=%fused_computation.23 | convolution fusion | flops 4843634688 | bytes 25690112 | tf_op jit(solution)/shard_map/rjf,jfd->rjd/dot_general | solution.py:133
  304.6 131.7 %while.15 = (s32[]{:T(128)}, f32[1024,1,1]{0,2,1:T(1,128)S(1)}, f32[1024,1,1]{0,2,1:T(1,128)S(1)}, f32[1024,1,1,64]{0,3,2,1:T(8,128)S(1)}, bf16[16,1024,1,128]{3...) while((s32[]{:T(128)}, f32[1024,1,1]{0,2,1:T(1,128)S(1)}, ...), condition=%wide.region_6.7_spmd.clone, body=%wide.region_3.6_spmd.clone.sunk | while | flops 277025792 | bytes 31129728 | solution.py:74
  304.6 1.0 dynamic-slice_bitcast_fusion.2
  305.6 2.8 multiply_reduce_fusion.4
  308.3 3.1 fusion.81
  312.8 1.0 dynamic-slice_bitcast_fusion.2
  313.8 2.8 multiply_reduce_fusion.4
  316.5 3.2 fusion.81
  321.1 1.0 dynamic-slice_bitcast_fusion.2
  322.1 2.8 multiply_reduce_fusion.4
  324.9 3.1 fusion.81
  329.4 1.0 dynamic-slice_bitcast_fusion.2
  330.4 2.8 multiply_reduce_fusion.4
  333.2 3.2 fusion.81
  337.8 1.0 dynamic-slice_bitcast_fusion.2
  338.7 2.8 multiply_reduce_fusion.4
  341.5 3.2 fusion.81
  346.1 1.0 dynamic-slice_bitcast_fusion.2
  347.1 2.8 multiply_reduce_fusion.4
  349.8 3.2 fusion.81
  354.4 1.0 dynamic-slice_bitcast_fusion.2
  355.4 2.8 multiply_reduce_fusion.4
  358.2 3.2 fusion.81
  362.7 1.0 dynamic-slice_bitcast_fusion.2
  363.7 2.8 multiply_reduce_fusion.4
  366.5 3.1 fusion.81
  372.0 2.8 multiply_reduce_fusion.4
  374.8 3.1 fusion.81
  380.2 2.8 multiply_reduce_fusion.4
  382.9 3.1 fusion.81
  388.3 2.8 multiply_reduce_fusion.4
  391.1 3.1 fusion.81
  396.5 2.8 multiply_reduce_fusion.4
  399.2 3.1 fusion.81
  404.6 2.8 multiply_reduce_fusion.4
  407.4 3.1 fusion.81
  412.8 2.8 multiply_reduce_fusion.4
  415.5 3.1 fusion.81
  420.9 2.8 multiply_reduce_fusion.4
  423.7 3.1 fusion.81
  429.1 2.8 multiply_reduce_fusion.4
  431.8 3.1 fusion.81
  438.6 5.6 %all-to-all-start.1 = ((bf16[16,2,2048]{2,1,0:T(2,128)(2,1)}), bf16[16,2,2048]{2,1,0:T(2,128)(2,1)S(1)}, u32[]{:S(2)}, u32[]{:S(2)}) async-start(bf16[16,2,2048]{2,1,0:T(2,128)(2,1)} %reshape.592), calls=%async_computation.1 | async-start | bytes 262144 | tf_op jit(solution)/shard_map/all_to_all | solution.py:122
  444.6 2.5 copy.153
  447.1 6.0 %all-to-all-done.1 = bf16[16,2,2048]{2,1,0:T(2,128)(2,1)S(1)} async-done(((bf16[16,2,2048]{2,1,0:T(2,128)(2,1)}), bf16[16,2,2048]{2,1,0:T(2,128)(2,1)S(1)}, u32[]{:S(2)}, u32[]{:S(2)}) %all-to-all-start.1) | async-done | bytes 131104 | tf_op jit(solution)/shard_map/all_to_all | solution.py:122
  453.0 3.8 all-to-all-start.4
  458.4 2.9 fusion.20
  461.2 7.9 %all-to-all-done.4 = bf16[16,9,2,1024]{3,2,1,0:T(2,128)(2,1)S(1)} async-done(((bf16[16,9,2,1024]{3,2,1,0:T(2,128)(2,1)}), bf16[16,9,2,1024]{3,2,1,0:T(2,128)(2,1)S(1)}, u32[]{:S(2)}, u32[]{:S(2)}) %all-to-all-start.4) | async-done | bytes 589856 | tf_op jit(solution)/shard_map/all_to_all | solution.py:181
  469.4 1.2 gather_fusion
  470.8 2.4 multiply_reduce_fusion.1
  (193 shorter events, 42.4 us)
Async XLA Ops:
  8.0 16.3 %copy-start = (bf16[1024,1024]{1,0:T(8,128)(2,1)S(1)}, bf16[1024,1024]{1,0:T(8,128)(2,1)}, u32[]{:S(2)}) copy-start(bf16[1024,1024]{1,0:T(8,128)(2,1)} %param.19) | copy-start | bytes 6291460
  8.0 14.2 %copy-start.3 = (bf16[64,1,1024]{2,0,1:T(8,128)(2,1)S(1)}, bf16[64,1,1024]{2,0,1:T(8,128)(2,1)}, u32[]{:S(2)}) copy-start(bf16[64,1,1024]{2,0,1:T(8,128)(2,1)} %param.17) | copy-start | bytes 393220
  8.0 14.4 %copy-start.5 = (f32[1024]{0:T(1024)S(1)}, f32[1024]{0:T(1024)}, u32[]{:S(2)}) copy-start(f32[1024]{0:T(1024)} %param.18) | copy-start | bytes 12292
  8.0 14.4 %copy-start.4 = (bf16[1024,256]{1,0:T(8,128)(2,1)S(1)}, bf16[1024,256]{1,0:T(8,128)(2,1)}, u32[]{:S(2)}) copy-start(bf16[1024,256]{1,0:T(8,128)(2,1)} %param.20) | copy-start | bytes 1572868
  14.7 18.7 %all-to-all-start.2 = ((bf16[16,9,2,1024]{3,2,1,0:T(2,128)(2,1)}), bf16[16,9,2,1024]{3,2,1,0:T(2,128)(2,1)S(1)}, u32[]{:S(2)}, u32[]{:S(2)}) async-start(bf16[16,9,2,1024]{3,2,1,0:T(2,128)(2,1)} %reshape.573), calls=%async_computation.2 | async-start | bytes 1179648 | tf_op jit(solution)/shard_map/all_to_all | solution.py:167
  33.4 27.7 %all-to-all-start = ((bf16[64,1,16,192]{3,0,1,2:T(8,128)(2,1)}), bf16[64,1,16,192]{3,0,1,2:T(8,128)(2,1)S(1)}, u32[]{:S(2)}, u32[]{:S(2)}) async-start(bf16[64,1,16,192]{3,0,1,2:T(8,128)(2,1)} %pad_maximum_fusion), calls=%async_computation | async-start | bytes 1048576 | tf_op jit(solution)/shard_map/all_to_all | solution.py:97
  66.0 4.9 %copy-start.8 = (f32[64]{0:T(128)S(1)}, f32[64]{0:T(128)}, u32[]{:S(2)}) copy-start(f32[64]{0:T(128)} %param.23) | copy-start | bytes 772
  66.0 209.4 %all-to-all-start.3 = ((bf16[16,144,2,1024]{3,1,2,0:T(8,128)(2,1)}), bf16[16,144,2,1024]{3,1,2,0:T(8,128)(2,1)}, u32[]{:S(2)}, u32[]{:S(2)}) async-start(bf16[16,144,2,1024]{3,1,2,0:T(8,128)(2,1)} %stack.23), calls=%async_computation.3 | async-start | bytes 18874368 | tf_op jit(solution)/shard_map/all_to_all | solution.py:174
  70.8 3.1 copy-start.7
  70.8 233.7 %all-gather.2.cloned.1.call-start = ((), (), s32[]{:S(2)}) async-start(), calls=%async_computation.6 | async-start | bytes 4456448 | tf_op jit(solution)/shard_map/all_gather | solution.py:115
  73.4 371.1 %reduce-scatter.2.cloned.1.call-start = ((), (), s32[]{:S(2)}) async-start(), calls=%async_computation.7 | async-start | bytes 10027008 | tf_op jit(solution)/shard_map/reduce_scatter | solution.py:177
  74.6 209.9 %copy-start.9 = (bf16[2,1024,256]{2,1,0:T(8,128)(2,1)S(1)}, bf16[2,1024,256]{2,1,0:T(8,128)(2,1)}, u32[]{:S(2)}) copy-start(bf16[2,1024,256]{2,1,0:T(8,128)(2,1)} %param.29) | copy-start | bytes 3145732
  304.6 139.9 %copy-start.6 = (f32[128,2]{0,1:T(2,128)S(1)}, f32[128,2]{0,1:T(2,128)}, u32[]{:S(2)}) copy-start(f32[128,2]{0,1:T(2,128)} %param.28) | copy-start | bytes 3076
  308.3 3.5 copy-start.2
  316.5 3.6 copy-start.2
  324.9 3.6 copy-start.2
  333.2 3.6 copy-start.2
  341.5 3.6 copy-start.2
  349.8 3.6 copy-start.2
  358.2 3.6 copy-start.2
  366.5 3.6 copy-start.2
  374.8 3.4 copy-start.2
  382.9 3.4 copy-start.2
  391.1 3.4 copy-start.2
  399.2 3.4 copy-start.2
  407.4 3.4 copy-start.2
  415.5 3.4 copy-start.2
  423.7 3.4 copy-start.2
  431.8 3.4 copy-start.2
  438.6 14.5 %all-to-all-start.1 = ((bf16[16,2,2048]{2,1,0:T(2,128)(2,1)}), bf16[16,2,2048]{2,1,0:T(2,128)(2,1)S(1)}, u32[]{:S(2)}, u32[]{:S(2)}) async-start(bf16[16,2,2048]{2,1,0:T(2,128)(2,1)} %reshape.592), calls=%async_computation.1 | async-start | bytes 262144 | tf_op jit(solution)/shard_map/all_to_all | solution.py:122
  453.0 16.1 %all-to-all-start.4 = ((bf16[16,9,2,1024]{3,2,1,0:T(2,128)(2,1)}), bf16[16,9,2,1024]{3,2,1,0:T(2,128)(2,1)S(1)}, u32[]{:S(2)}, u32[]{:S(2)}) async-start(bf16[16,9,2,1024]{3,2,1,0:T(2,128)(2,1)} %bitcast.25), calls=%async_computation.5 | async-start | bytes 1179648 | tf_op jit(solution)/shard_map/all_to_all | solution.py:181
  458.3 14.8 %copy-start.1 = (bf16[1024,1024]{1,0:T(8,128)(2,1)S(1)}, bf16[1024,1024]{1,0:T(8,128)(2,1)}, u32[]{:S(2)}) copy-start(bf16[1024,1024]{1,0:T(8,128)(2,1)} %param.19) | copy-start | bytes 6291460
Sparse Core Ops, SparseCore 0:
  74.6 52.0 all-gather.1
Sparse Core Ops, SparseCore 1:
  304.6 65.5 reduce-scatter.1
